TPU v7x, 32 devices: a whole 2x2x4 slice. The times are simulated.
32 devices in a mesh: sp: 8 (over z, y), tp: 4 (over x, core).
Axes of the slice: x: 2, y: 2, z: 4, core: 2. Of those that a mesh axis runs over, the one named last changes fastest.
Arguments:
- gate_in: bfloat16 [4096, 2048], P('sp', 'tp'), may hold values from -6 to 6
- value_in: bfloat16 [4096, 2048], P('sp', 'tp'), may hold values from -6 to 6
- gate_out: bfloat16 [4096, 2048], P('sp', 'tp'), may hold values from -6 to 6
- conv_taps: float32 [3, 2048], P(None, 'tp'), may hold values from -3.5 to 3.5
- proj_weight: bfloat16 [2048, 2048], P('tp'), may hold values from -0.125 to 0.125
- residual: bfloat16 [4096, 2048], P(('sp', 'tp')), may hold values from -6 to 6
- norm_gain: float32 [2048], replicated, may hold values from 0.1 to 1.9
- routes: int32 [4096, 2], P('sp'), may hold values from 0 to 7, all different within a row; in each aligned block of 128 rows (0 to 127, 128 to 255, ...) at most 64 rows name the same one
- route_weight: float32 [4096, 2], P('sp'), may hold values from 0.1 to 0.9
- expert_gate: bfloat16 [8, 2048, 2048], P('sp', None, 'tp'), may hold values from -0.125 to 0.125
- expert_up: bfloat16 [8, 2048, 2048], P('sp', None, 'tp'), may hold values from -0.125 to 0.125
- expert_down: bfloat16 [8, 2048, 2048], P('sp', 'tp'), may hold values from -0.125 to 0.125
Outputs:
- layer_out: bfloat16 [4096, 2048], P(('sp', 'tp'))
Inputs may be any that keep to these rules, and one draw needn't show every extreme that they name: `routes`: A token's 2 experts differ. In each aligned block of 128 tokens no expert is named by more than 64 tokens, a bound that some block reaches.
All inputs are finite; a program needn't handle non-finite values.
Results may differ from a plain program's by a relative error of at most 0.012.
Values may be sent and summed in bfloat16 or wider, within the bound.
A program may use at most 128 MiB of HBM per device.

v0:
```python
import jax
import jax.numpy as jnp
from jax import lax
from jax.sharding import PartitionSpec as P


def passed_along(shard, axis, by):
    size = lax.axis_size(axis)
    pairs = [(i, i + by) for i in range(size) if 0 <= i + by < size]
    return lax.ppermute(shard, axis, pairs)


def rounded(values):
    return lax.optimization_barrier(values.astype(jnp.bfloat16)).astype(jnp.float32)


def slot_numbers(route_ids, block_rows, expert_count):
    block_count = route_ids.shape[0] // block_rows
    flat_ids = route_ids.reshape(block_count, block_rows * route_ids.shape[1])
    one_hot = (
        flat_ids[:, :, None] == jnp.arange(expert_count, dtype=jnp.int32)[None, None, :]
    ).astype(jnp.int32)
    before = jnp.cumsum(one_hot, axis=1) - one_hot
    return jnp.sum(before * one_hot, axis=2).reshape(route_ids.shape)


def normalize(hidden_rows, norm_gain):
    inverse = lax.rsqrt(jnp.mean(hidden_rows * hidden_rows, axis=-1, keepdims=True) + 1e-05)
    return (hidden_rows * inverse * norm_gain).astype(jnp.bfloat16)


def dispatch_rows(normed, route_ids, block_rows, expert_count, capacity):
    row_count = route_ids.shape[0]
    top_count = route_ids.shape[1]
    block_count = row_count // block_rows
    slots = slot_numbers(route_ids, block_rows, expert_count)
    row_ids = jnp.arange(row_count, dtype=jnp.int32)
    flat_index = ((row_ids // block_rows)[:, None] * expert_count + route_ids) * capacity + slots
    slot_token = (
        jnp.full((block_count * expert_count * capacity,), row_count, jnp.int32)
        .at[flat_index.reshape(-1)]
        .set(jnp.repeat(row_ids, top_count))
    )
    padded_rows = jnp.concatenate([normed, jnp.zeros((1, normed.shape[1]), jnp.bfloat16)], axis=0)
    outgoing = padded_rows[slot_token].reshape(block_count, expert_count, capacity, normed.shape[1])
    return (outgoing, slots)


def body(
    gate_in,
    value_in,
    gate_out,
    conv_taps,
    proj_weight,
    residual,
    norm_gain,
    routes,
    route_weight,
    expert_gate,
    expert_up,
    expert_down,
):
    tok_dev = gate_in.shape[0]
    model_width = residual.shape[1]
    tp_count = lax.axis_size("tp")
    groups = lax.axis_size("sp")
    quarter = residual.shape[0]
    top_count = routes.shape[1]
    capacity = 2 * quarter * top_count // groups
    tp_index = lax.axis_index("tp")
    first_own = tp_index * quarter
    prior_gate, prior_value = passed_along(
        (gate_in[tok_dev - 2 :], value_in[tok_dev - 2 :]), "sp", 1
    )
    product = gate_in.astype(jnp.float32) * value_in.astype(jnp.float32)
    prior_mix = prior_gate.astype(jnp.float32) * prior_value.astype(jnp.float32)
    padded = jnp.concatenate([prior_mix, product], axis=0)
    conv_sum = conv_taps[0] * padded[:-2] + conv_taps[1] * padded[1:-1] + conv_taps[2] * padded[2:]
    mixed_out = (gate_out.astype(jnp.float32) * conv_sum).astype(jnp.bfloat16)
    own_routes = lax.dynamic_slice_in_dim(routes, first_own, quarter, 0)
    own_weights = lax.dynamic_slice_in_dim(route_weight, first_own, quarter, 0)
    row_block = mixed_out
    summed = lax.psum_scatter(
        rounded(jnp.dot(row_block, proj_weight, preferred_element_type=jnp.float32)).astype(
            jnp.bfloat16
        ),
        "tp",
        scatter_dimension=0,
        tiled=True,
    ).astype(jnp.float32)
    my_rows = residual.astype(jnp.float32) + summed
    normed = normalize(my_rows, norm_gain)
    outgoing, own_slots = dispatch_rows(normed, own_routes, quarter, groups, capacity)
    own_arrived = lax.all_to_all(outgoing, "sp", split_axis=1, concat_axis=1, tiled=True)
    received = lax.all_gather(own_arrived, "tp", axis=0, tiled=True)
    flat_rows = received.reshape(tp_count * groups * capacity, model_width)
    gate_weight = expert_gate[0]
    up_weight = expert_up[0]
    down_weight = expert_down[0]
    row_block = flat_rows
    gate_pre = jnp.dot(row_block, gate_weight, preferred_element_type=jnp.float32)
    up_pre = jnp.dot(row_block, up_weight, preferred_element_type=jnp.float32)
    hidden = (jax.nn.silu(gate_pre) * up_pre).astype(jnp.bfloat16)
    expert_rows = lax.psum_scatter(
        rounded(jnp.dot(hidden, down_weight, preferred_element_type=jnp.float32)).astype(
            jnp.bfloat16
        ),
        "tp",
        scatter_dimension=0,
        tiled=True,
    )
    returned = lax.all_to_all(
        expert_rows.reshape(groups, capacity, model_width),
        "sp",
        split_axis=0,
        concat_axis=0,
        tiled=True,
    )
    flat_pick = own_routes * capacity + own_slots
    picked = returned.reshape(groups * capacity, model_width)[flat_pick]
    weighted = jnp.sum(own_weights[:, :, None] * picked.astype(jnp.float32), axis=1)
    return (my_rows + weighted).astype(jnp.bfloat16)


def solution(mesh):
    placed = (
        P("sp", "tp"),
        P("sp", "tp"),
        P("sp", "tp"),
        P(None, "tp"),
        P("tp", None),
        P(("sp", "tp"), None),
        P(),
        P("sp", None),
        P("sp", None),
        P("sp", None, "tp"),
        P("sp", None, "tp"),
        P("sp", "tp", None),
    )
    return jax.shard_map(
        body, mesh=mesh, in_specs=placed, out_specs=P(("sp", "tp"), None), check_vma=False
    )
```

profile of v0, /device:TPU:0, one launch (start us, length us, event | category | flops | bytes accessed | tf_op | source)
XLA Modules:
  0.0 337.2 jit_solution(5291792366952498572)
XLA Ops:
  6.5 0.9 slice.28
  7.4 5.0 %collective-permute-start = (bf16[2,512]{1,0:T(2,128)(2,1)S(1)}, bf16[2,512]{1,0:T(2,128)(2,1)S(1)}, u32[]{:S(2)}, u32[]{:S(2)}) collective-permute-start(bf16[2,512]{1,0:T(2,128)(2,1)S(1)} %slice.28), channel_id=1, source_target_pairs={{0,4},{4,8},{8,12},{12,16},{16,20},{20,24},{24,28},{1,5},{5,9},{9,... | collective-permute-start | bytes 6152 | tf_op jit(solution)/shard_map/ppermute | solution.py:10
  12.4 0.7 slice.29
  13.1 3.4 %collective-permute-start.1 = (bf16[2,512]{1,0:T(2,128)(2,1)S(1)}, bf16[2,512]{1,0:T(2,128)(2,1)S(1)}, u32[]{:S(2)}, u32[]{:S(2)}) collective-permute-start(bf16[2,512]{1,0:T(2,128)(2,1)S(1)} %slice.29), channel_id=1, source_target_pairs={{0,4},{4,8},{8,12},{12,16},{16,20},{20,24},{24,28},{1,5},{5,9},{9,... | collective-permute-start | bytes 6152 | tf_op jit(solution)/shard_map/ppermute | solution.py:10
  16.6 1.3 convert_multiply_fusion
  18.0 3.8 %convolution_convert_fusion.1 = bf16[512,2048]{1,0:T(8,128)(2,1)} fusion(bf16[512,2048]{1,0:T(8,128)(2,1)S(1)} %copy-done.6, f32[2,512]{1,0:T(2,128)S(1)} %convert_multiply_fusion.1, f32[512,512]{1,0:T(8,128)S(1)} %convert_multiply_fusion, bf16[512,512]{1,0:T(8,128)(2,1)} %param.14, f32[512]{0:T(512)S(1)} %bitcast.44, f32[512]{0:T(512)S(1)} %bitcast.45, ...), kind=kOutput, calls=%fused_computation.5 | convolution fusion | flops 1077411840 | bytes 5777408 | tf_op jit(solution)/shard_map/dot_general | solution.py:84
  21.9 0.7 constant_dynamic-slice_fusion
  22.7 0.1 eq.27
  22.9 0.6 reduce-window.6
  23.5 0.2 slice_reduce_fusion
  23.8 0.1 reshape.195
  24.1 0.1 reshape.196
  24.2 0.1 reshape.222
  24.4 1.4 scatter_custom_fusion
  25.8 29.2 %reduce-scatter.3.cloned.1.call-done = bf16[128,2048]{1,0:T(8,128)(2,1)} async-done(((bf16[512,2048]{1,0:T(8,128)(2,1)}), bf16[128,2048]{1,0:T(8,128)(2,1)}) %reduce-scatter.3.cloned.1.call-update) | async-done | bytes 524304 | tf_op jit(solution)/shard_map/reduce_scatter | solution.py:83
  55.0 1.3 multiply_reduce_fusion.1
  56.3 1.3 multiply_convert_fusion.1
  57.6 3.3 gather_fusion
  61.0 53.7 %all_to_all.10 = bf16[1,8,64,2048]{3,2,0,1:T(8,128)(2,1)} all-to-all(bf16[1,8,64,2048]{3,2,0,1:T(8,128)(2,1)} %bitcast.39), channel_id=1, replica_groups=mesh['sp'=8,'tp'=4] {'sp'}, dimensions={1} | all-to-all | bytes 4194304 | tf_op jit(solution)/shard_map/all_to_all | solution.py:94
  114.8 56.4 %all-gather.2.cloned.1.call-done = bf16[4,8,64,2048]{3,2,1,0:T(8,128)(2,1)} async-done(((bf16[1,8,64,2048]{3,2,1,0:T(8,128)(2,1)}), bf16[4,8,64,2048]{3,2,1,0:T(8,128)(2,1)}) %all-gather.2.cloned.1.call-update) | async-done | bytes 8388624 | tf_op jit(solution)/shard_map/all_gather | solution.py:95
  171.2 7.7 %fusion.2 = f32[2048,512]{1,0:T(8,128)S(1)} fusion(bf16[2048,2048]{1,0:T(8,128)(2,1)} %bitcast.47, bf16[1,2048,512]{2,1,0:T(8,128)(2,1)} %param.21), kind=kOutput, calls=%fused_computation.8 | convolution fusion | flops 4294967296 | bytes 14680064 | tf_op jit(solution)/shard_map/dot_general | solution.py:101
  178.9 5.2 %multiply_convert_fusion = bf16[2048,512]{1,0:T(8,128)(2,1)S(1)} fusion(f32[2048,512]{1,0:T(8,128)S(1)} %fusion.2, bf16[2048,2048]{1,0:T(8,128)(2,1)S(1)} %bitcast.48, bf16[1,2048,512]{2,1,0:T(8,128)(2,1)S(1)} %copy-done.7), kind=kOutput, calls=%fused_computation.4 | convolution fusion | flops 4301258752 | bytes 16777216 | tf_op jit(solution)/shard_map/dot_general | solution.py:102
  184.1 6.8 %convolution_convert_fusion = bf16[2048,2048]{1,0:T(8,128)(2,1)} fusion(bf16[2048,512]{1,0:T(8,128)(2,1)S(1)} %multiply_convert_fusion, bf16[1,512,2048]{2,1,0:T(8,128)(2,1)S(1)} %copy-done), kind=kOutput, calls=%fused_computation.3 | convolution fusion | flops 4299161600 | bytes 12582912 | tf_op jit(solution)/shard_map/dot_general | solution.py:105
  190.9 71.5 %reduce-scatter.5.cloned.1.call-done = bf16[512,2048]{1,0:T(8,128)(2,1)} async-done(((bf16[2048,2048]{1,0:T(8,128)(2,1)}), bf16[512,2048]{1,0:T(8,128)(2,1)}) %reduce-scatter.5.cloned.1.call-update) | async-done | bytes 2097168 | tf_op jit(solution)/shard_map/reduce_scatter | solution.py:104
  262.5 5.5 %all-to-all-start.1 = ((bf16[8,64,2048]{2,1,0:T(8,128)(2,1)}), bf16[8,64,2048]{2,1,0:T(8,128)(2,1)}, u32[]{:S(2)}, u32[]{:S(2)}) async-start(bf16[8,64,2048]{2,1,0:T(8,128)(2,1)} %bitcast.41), calls=%async_computation.3 | async-start | bytes 4194304 | tf_op jit(solution)/shard_map/all_to_all | solution.py:112
  268.0 0.1 reshape.212
  268.1 0.7 constant_dynamic-slice_fusion.1
  268.9 47.2 %all-to-all-done.1 = bf16[8,64,2048]{2,1,0:T(8,128)(2,1)} async-done(((bf16[8,64,2048]{2,1,0:T(8,128)(2,1)}), bf16[8,64,2048]{2,1,0:T(8,128)(2,1)}, u32[]{:S(2)}, u32[]{:S(2)}) %all-to-all-start.1) | async-done | bytes 2097184 | tf_op jit(solution)/shard_map/all_to_all | solution.py:112
  316.2 5.2 %gather_fusion.1 = bf16[256,2048]{1,0:T(8,128)(2,1)} fusion(bf16[512,2048]{1,0:T(8,128)(2,1)} %bitcast.18, s32[1024]{0:T(1024)S(1)} %pad_clamp_fusion), kind=kCustom, calls=%fused_computation.1 | custom fusion | bytes 2098176 | tf_op jit(solution)/shard_map/gather | solution.py:120
  321.4 3.4 %reshape.229 = f32[128,2,2048]{2,1,0:T(2,128)} reshape(bf16[256,2048]{1,0:T(8,128)(2,1)} %gather_fusion.1) | data formatting | bytes 3145728 | tf_op jit(solution)/shard_map/convert_element_type | solution.py:121
  324.8 4.9 %multiply_reduce_fusion = f32[128,2048]{1,0:T(8,128)S(1)} fusion(f32[128,2,2048]{2,1,0:T(2,128)} %reshape.229, f32[128,2]{1,0:T(8,128)S(1)} %copy.16), kind=kLoop, calls=%fused_computation.10 | loop fusion | flops 786432 | bytes 3146752 | tf_op jit(solution)/shard_map/reduce_sum | solution.py:121
  329.7 1.0 add_convert_fusion
  (41 shorter events, 0.7 us)
Async XLA Ops:
  6.5 177.6 %copy-start = (bf16[1,512,2048]{2,1,0:T(8,128)(2,1)S(1)}, bf16[1,512,2048]{2,1,0:T(8,128)(2,1)}, u32[]{:S(2)}) copy-start(bf16[1,512,2048]{2,1,0:T(8,128)(2,1)} %param.23) | copy-start | bytes 6291460
  6.5 11.4 %copy-start.4 = (f32[3,512]{1,0:T(4,128)S(1)}, f32[3,512]{1,0:T(4,128)}, u32[]{:S(2)}) copy-start(f32[3,512]{1,0:T(4,128)} %param.15) | copy-start | bytes 18436
  6.5 48.5 %reduce-scatter.3.cloned.1.call-start = ((), (), s32[]{:S(2)}) async-start(), calls=%async_computation.4 | async-start | bytes 2621440 | tf_op jit(solution)/shard_map/reduce_scatter | solution.py:83
  6.5 11.4 %copy-start.6 = (bf16[512,2048]{1,0:T(8,128)(2,1)S(1)}, bf16[512,2048]{1,0:T(8,128)(2,1)}, u32[]{:S(2)}) copy-start(bf16[512,2048]{1,0:T(8,128)(2,1)} %param.16) | copy-start | bytes 6291460
  7.4 10.5 %collective-permute-start = (bf16[2,512]{1,0:T(2,128)(2,1)S(1)}, bf16[2,512]{1,0:T(2,128)(2,1)S(1)}, u32[]{:S(2)}, u32[]{:S(2)}) collective-permute-start(bf16[2,512]{1,0:T(2,128)(2,1)S(1)} %slice.28), channel_id=1, source_target_pairs={{0,4},{4,8},{8,12},{12,16},{16,20},{20,24},{24,28},{1,5},{5,9},{9,... | collective-permute-start | bytes 6152 | tf_op jit(solution)/shard_map/ppermute | solution.py:10
  13.1 4.8 %collective-permute-start.1 = (bf16[2,512]{1,0:T(2,128)(2,1)S(1)}, bf16[2,512]{1,0:T(2,128)(2,1)S(1)}, u32[]{:S(2)}, u32[]{:S(2)}) collective-permute-start(bf16[2,512]{1,0:T(2,128)(2,1)S(1)} %slice.29), channel_id=1, source_target_pairs={{0,4},{4,8},{8,12},{12,16},{16,20},{20,24},{24,28},{1,5},{5,9},{9,... | collective-permute-start | bytes 6152 | tf_op jit(solution)/shard_map/ppermute | solution.py:10
  21.8 33.2 %copy-start.1 = (bf16[128,2048]{1,0:T(8,128)(2,1)S(1)}, bf16[128,2048]{1,0:T(8,128)(2,1)}, u32[]{:S(2)}) copy-start(bf16[128,2048]{1,0:T(8,128)(2,1)} %param.17) | copy-start | bytes 1572868
  21.8 34.5 %copy-start.3 = (f32[2048]{0:T(1024)S(1)}, f32[2048]{0:T(1024)}, u32[]{:S(2)}) copy-start(f32[2048]{0:T(1024)} %param.18) | copy-start | bytes 24580
  21.8 149.4 %all-gather.2.cloned.1.call-start = ((), (), s32[]{:S(2)}) async-start(), calls=%async_computation.5 | async-start | bytes 10485760 | tf_op jit(solution)/shard_map/all_gather | solution.py:95
  114.7 147.8 %reduce-scatter.5.cloned.1.call-start = ((), (), s32[]{:S(2)}) async-start(), calls=%async_computation.6 | async-start | bytes 10485760 | tf_op jit(solution)/shard_map/reduce_scatter | solution.py:104
  171.2 7.7 %copy-start.5 = (bf16[4,8,64,2048]{3,2,1,0:T(8,128)(2,1)S(1)}, bf16[4,8,64,2048]{3,2,1,0:T(8,128)(2,1)}, u32[]{:S(2)}) copy-start(bf16[4,8,64,2048]{3,2,1,0:T(8,128)(2,1)} %all-gather.2.cloned.1.call-done) | copy-start | bytes 25165828
  171.2 7.7 %copy-start.7 = (bf16[1,2048,512]{2,1,0:T(8,128)(2,1)S(1)}, bf16[1,2048,512]{2,1,0:T(8,128)(2,1)}, u32[]{:S(2)}) copy-start(bf16[1,2048,512]{2,1,0:T(8,128)(2,1)} %param.22) | copy-start | bytes 6291460
  262.5 53.7 %all-to-all-start.1 = ((bf16[8,64,2048]{2,1,0:T(8,128)(2,1)}), bf16[8,64,2048]{2,1,0:T(8,128)(2,1)}, u32[]{:S(2)}, u32[]{:S(2)}) async-start(bf16[8,64,2048]{2,1,0:T(8,128)(2,1)} %bitcast.41), calls=%async_computation.3 | async-start | bytes 4194304 | tf_op jit(solution)/shard_map/all_to_all | solution.py:112
  324.8 4.9 %copy-start.2 = (bf16[128,2048]{1,0:T(8,128)(2,1)S(1)}, bf16[128,2048]{1,0:T(8,128)(2,1)}, u32[]{:S(2)}) copy-start(bf16[128,2048]{1,0:T(8,128)(2,1)} %reduce-scatter.3.cloned.1.call-done) | copy-start | bytes 1572868
Sparse Core Ops, SparseCore 0:
  22.0 32.9 reduce-scatter.2
  114.8 56.3 all-gather.1
  191.0 71.3 reduce-scatter.4
where the time goes:
time: 338 us; the launch traced here: 337 us
  waiting for transfers between devices  204 us (60%)
  blocking collectives  53.7 us (16%)
  matrix products  23.5 us (7%)
  local copies, waits for them, and re-layouts  17.5 us (5%)
  starting transfers between devices  14 us (4%)
  between operations  13.3 us (4%)
  other arithmetic  10.6 us (3%)
    reduce_scatter x1, waiting for transfers between devices, body(): lax.psum_scatter(rounded(jnp.dot(hidden, down_weight, preferred_element_t...  71.5 us
    all_gather x1, waiting for transfers between devices, body(): received = lax.all_gather(own_arrived, 'tp', axis=0, tiled=True)  56.4 us
    all_to_all x1, blocking collectives, body(): lax.all_to_all(outgoing, 'sp', split_axis=1, concat_axis=1, tiled=True)  53.7 us
    all_to_all x1, waiting for transfers between devices, body(): lax.all_to_all(expert_rows.reshape(groups, capacity, model_width), 'sp',...  47.2 us
    reduce_scatter x1, waiting for transfers between devices, body(): lax.psum_scatter(rounded(jnp.dot(row_block, proj_weight, preferred_elemen...  29.2 us
    ppermute x2, starting transfers between devices, passed_along(): return lax.ppermute(shard, axis, pairs)  8.43 us
    dot_general x1, matrix products, body(): jnp.dot(row_block, gate_weight, preferred_element_type=jnp.float32)  7.67 us
    dot_general x1, matrix products, body(): jnp.dot(hidden, down_weight, preferred_element_type=jnp.float32)  6.79 us
  transfers between devices with their start and end apart: 6, of which 4 were waited for; matrix products, arithmetic and copies ran while one was open for 2% of the time, Pallas kernels for 0%

commit v1 on v0

--- a/solution.py
+++ b/solution.py
@@ -2,6 +2,16 @@
 import jax.numpy as jnp
 from jax import lax
 from jax.sharding import PartitionSpec as P
+
+
+def turned_line(array, axis, dim):
+    devices = lax.axis_size(axis)
+    held, tiles = (array, [array])
+    for _ in range(devices - 1):
+        held = lax.ppermute(held, axis, [(i, (i + 1) % devices) for i in range(devices)])
+        tiles.insert(0, held)
+    line = jnp.concatenate(tiles, axis=dim)
+    return jnp.roll(line, (lax.axis_index(axis) + 1) * array.shape[dim], axis=dim)
 
 
 def passed_along(shard, axis, by):
@@ -92,7 +102,7 @@
     normed = normalize(my_rows, norm_gain)
     outgoing, own_slots = dispatch_rows(normed, own_routes, quarter, groups, capacity)
     own_arrived = lax.all_to_all(outgoing, "sp", split_axis=1, concat_axis=1, tiled=True)
-    received = lax.all_gather(own_arrived, "tp", axis=0, tiled=True)
+    received = turned_line(own_arrived, "tp", 0)
     flat_rows = received.reshape(tp_count * groups * capacity, model_width)
     gate_weight = expert_gate[0]
     up_weight = expert_up[0]

time: 338 us -> 387 us (1.14)
  local copies, waits for them, and re-layouts: 17.5 us -> 48.2 us
  waiting for transfers between devices: 204 us -> 222 us
    ppermute x0 -> x3, waiting for transfers between devices: none -> 76.8 us  [turned_line(): lax.ppermute(held, axis, [(i, (i + 1) % devices) for i in range(devices)])]
    all_gather x1 -> x0, waiting for transfers between devices: 56.4 us -> none  [body(): received = lax.all_gather(own_arrived, 'tp', axis=0, tiled=True)]
    unnamed x17 -> x30, local copies, waits for them, and re-layouts: 0.15 us -> 20.1 us
    dynamic_slice x0 -> x1, local copies, waits for them, and re-layouts: none -> 8.41 us  [turned_line(): jnp.roll(line, (lax.axis_index(axis) + 1) * array.shape[dim], axis=dim)]
  transfers between devices with their start and end apart: 6 -> 8, of which waited for: 4 -> 6; matrix products, arithmetic and copies ran while one was open for 2% -> 2% of each run, Pallas kernels for 0% -> 0%
where the time goes in v1:
time: 387 us; the launch traced here: 386 us
  waiting for transfers between devices  222 us (57%)
  blocking collectives  53.6 us (14%)
  local copies, waits for them, and re-layouts  48.2 us (12%)
  matrix products  24.1 us (6%)
  starting transfers between devices  13.9 us (4%)
  between operations  13.6 us (4%)
  other arithmetic  10.6 us (3%)
    ppermute x3, waiting for transfers between devices, turned_line(): lax.ppermute(held, axis, [(i, (i + 1) % devices) for i in range(devices)])  76.8 us
    reduce_scatter x1, waiting for transfers between devices, body(): lax.psum_scatter(rounded(jnp.dot(hidden, down_weight, preferred_element_t...  69.6 us
    all_to_all x1, blocking collectives, body(): lax.all_to_all(outgoing, 'sp', split_axis=1, concat_axis=1, tiled=True)  53.6 us
    all_to_all x1, waiting for transfers between devices, body(): lax.all_to_all(expert_rows.reshape(groups, capacity, model_width), 'sp',...  47.2 us
    reduce_scatter x1, waiting for transfers between devices, body(): lax.psum_scatter(rounded(jnp.dot(row_block, proj_weight, preferred_elemen...  28.4 us
    unnamed x30, local copies, waits for them, and re-layouts  20.1 us
    dynamic_slice x1, local copies, waits for them, and re-layouts, turned_line(): jnp.roll(line, (lax.axis_index(axis) + 1) * array.shape[dim], axis=dim)  8.41 us
    ppermute x2, starting transfers between devices, passed_along(): return lax.ppermute(shard, axis, pairs)  8.3 us
  transfers between devices with their start and end apart: 8, of which 6 were waited for; matrix products, arithmetic and copies ran while one was open for 2% of the time, Pallas kernels for 0%

profile of v1, /device:TPU:0, one launch (start us, length us, event | category | flops | bytes accessed | tf_op | source)
XLA Modules:
  0.0 386.1 jit_solution(16566651305927072678)
XLA Ops:
  7.4 4.9 %collective-permute-start = (bf16[2,512]{1,0:T(2,128)(2,1)S(1)}, bf16[2,512]{1,0:T(2,128)(2,1)S(1)}, u32[]{:S(2)}, u32[]{:S(2)}) collective-permute-start(bf16[2,512]{1,0:T(2,128)(2,1)S(1)} %slice.28), channel_id=1, source_target_pairs={{0,4},{4,8},{8,12},{12,16},{16,20},{20,24},{24,28},{1,5},{5,9},{9,... | collective-permute-start | bytes 6152 | tf_op jit(solution)/shard_map/ppermute | solution.py:20
  13.0 3.4 collective-permute-start.1
  16.4 1.3 convert_multiply_fusion
  18.6 4.6 %convolution_convert_fusion.1 = bf16[512,2048]{1,0:T(8,128)(2,1)} fusion(bf16[512,2048]{1,0:T(8,128)(2,1)} %param.16, f32[2,512]{1,0:T(2,128)S(1)} %convert_multiply_fusion.1, f32[512,512]{1,0:T(8,128)S(1)} %convert_multiply_fusion, bf16[512,512]{1,0:T(8,128)(2,1)} %param.14, f32[512]{0:T(512)S(1)} %bitcast.50, f32[512]{0:T(512)S(1)} %bitcast.51, ...), kind=kOutput, calls=%fused_computation.5 | convolution fusion | flops 1077411840 | bytes 5777408 | tf_op jit(solution)/shard_map/dot_general | solution.py:94
  25.7 1.4 scatter_custom_fusion
  27.2 28.4 %reduce-scatter.3.cloned.1.call-done = bf16[128,2048]{1,0:T(8,128)(2,1)} async-done(((bf16[512,2048]{1,0:T(8,128)(2,1)}), bf16[128,2048]{1,0:T(8,128)(2,1)}) %reduce-scatter.3.cloned.1.call-update) | async-done | bytes 524304 | tf_op jit(solution)/shard_map/reduce_scatter | solution.py:93
  55.6 1.3 multiply_reduce_fusion.1
  58.2 3.3 gather_fusion
  61.6 53.6 %all_to_all.10 = bf16[1,8,64,2048]{3,2,0,1:T(8,128)(2,1)S(1)} all-to-all(bf16[1,8,64,2048]{3,2,0,1:T(8,128)(2,1)} %bitcast.46), channel_id=1, replica_groups=mesh['sp'=8,'tp'=4] {'sp'}, dimensions={1} | all-to-all | bytes 4194304 | tf_op jit(solution)/shard_map/all_to_all | solution.py:104
  115.2 1.3 copy-done.1
  116.5 25.5 %collective-permute-done.2 = bf16[1,8,64,2048]{3,2,1,0:T(8,128)(2,1)S(1)} collective-permute-done((bf16[1,8,64,2048]{3,2,1,0:T(8,128)(2,1)S(1)}, bf16[1,8,64,2048]{3,2,1,0:T(8,128)(2,1)S(1)}, u32[]{:S(2)}, u32[]{:S(2)}) %collective-permute-start.2) | collective-permute-done | bytes 2097184 | tf_op jit(solution)/shard_map/ppermute | solution.py:11
  141.9 1.3 copy-done.4
  143.3 25.6 %collective-permute-done.3 = bf16[1,8,64,2048]{3,2,1,0:T(8,128)(2,1)} collective-permute-done((bf16[1,8,64,2048]{3,2,1,0:T(8,128)(2,1)S(1)}, bf16[1,8,64,2048]{3,2,1,0:T(8,128)(2,1)}, u32[]{:S(2)}, u32[]{:S(2)}) %collective-permute-start.3) | collective-permute-done | bytes 2097184 | tf_op jit(solution)/shard_map/ppermute | solution.py:11
  168.8 25.8 %collective-permute-done.4 = bf16[1,8,64,2048]{3,2,1,0:T(8,128)(2,1)} collective-permute-done((bf16[1,8,64,2048]{3,2,1,0:T(8,128)(2,1)}, bf16[1,8,64,2048]{3,2,1,0:T(8,128)(2,1)}, u32[]{:S(2)}, u32[]{:S(2)}) %collective-permute-start.4) | collective-permute-done | bytes 2097184 | tf_op jit(solution)/shard_map/ppermute | solution.py:11
  194.6 3.2 constant_dynamic-update-slice_fusion.7
  197.8 3.3 constant_dynamic-update-slice_fusion.6
  201.1 1.5 constant_dynamic-update-slice_fusion.5
  202.6 1.5 constant_dynamic-update-slice_fusion.4
  204.0 3.2 constant_dynamic-update-slice_fusion.3
  207.3 3.1 constant_dynamic-update-slice_fusion.2
  210.4 1.5 constant_dynamic-update-slice_fusion.1
  211.9 1.5 constant_dynamic-update-slice_fusion
  213.4 8.4 %constant_dynamic-slice_fusion = bf16[4,8,64,2048]{3,2,1,0:T(8,128)(2,1)} fusion(bf16[8,8,64,2048]{3,2,1,0:T(8,128)(2,1)} %constant_dynamic-update-slice_fusion, s32[]{:T(128)S(6)} %select_n.47), kind=kLoop, calls=%fused_computation.58 | loop fusion | bytes 16777220 | tf_op jit(solution)/shard_map/jit(_roll_dynamic)/dynamic_slice | solution.py:14
  221.8 7.7 %fusion.2 = f32[2048,512]{1,0:T(8,128)S(1)} fusion(bf16[2048,2048]{1,0:T(8,128)(2,1)} %bitcast.44, bf16[1,2048,512]{2,1,0:T(8,128)(2,1)S(1)} %copy-done.9), kind=kOutput, calls=%fused_computation.8 | convolution fusion | flops 4294967296 | bytes 14680064 | tf_op jit(solution)/shard_map/dot_general | solution.py:111
  229.5 5.2 %multiply_convert_fusion = bf16[2048,512]{1,0:T(8,128)(2,1)S(1)} fusion(f32[2048,512]{1,0:T(8,128)S(1)} %fusion.2, bf16[2048,2048]{1,0:T(8,128)(2,1)S(1)} %bitcast.45, bf16[1,2048,512]{2,1,0:T(8,128)(2,1)S(1)} %copy-done.10), kind=kOutput, calls=%fused_computation.4 | convolution fusion | flops 4301258752 | bytes 16777216 | tf_op jit(solution)/shard_map/dot_general | solution.py:112
  234.7 6.7 %convolution_convert_fusion = bf16[2048,2048]{1,0:T(8,128)(2,1)} fusion(bf16[2048,512]{1,0:T(8,128)(2,1)S(1)} %multiply_convert_fusion, bf16[1,512,2048]{2,1,0:T(8,128)(2,1)S(1)} %copy-done), kind=kOutput, calls=%fused_computation.3 | convolution fusion | flops 4299161600 | bytes 12582912 | tf_op jit(solution)/shard_map/dot_general | solution.py:115
  241.4 69.6 %reduce-scatter.5.cloned.1.call-done = bf16[512,2048]{1,0:T(8,128)(2,1)} async-done(((bf16[2048,2048]{1,0:T(8,128)(2,1)}), bf16[512,2048]{1,0:T(8,128)(2,1)}) %reduce-scatter.5.cloned.1.call-update) | async-done | bytes 2097168 | tf_op jit(solution)/shard_map/reduce_scatter | solution.py:114
  311.0 5.5 %all-to-all-start.1 = ((bf16[8,64,2048]{2,1,0:T(8,128)(2,1)}), bf16[8,64,2048]{2,1,0:T(8,128)(2,1)}, u32[]{:S(2)}, u32[]{:S(2)}) async-start(bf16[8,64,2048]{2,1,0:T(8,128)(2,1)} %bitcast.47), calls=%async_computation.3 | async-start | bytes 4194304 | tf_op jit(solution)/shard_map/all_to_all | solution.py:122
  317.5 47.2 %all-to-all-done.1 = bf16[8,64,2048]{2,1,0:T(8,128)(2,1)} async-done(((bf16[8,64,2048]{2,1,0:T(8,128)(2,1)}), bf16[8,64,2048]{2,1,0:T(8,128)(2,1)}, u32[]{:S(2)}, u32[]{:S(2)}) %all-to-all-start.1) | async-done | bytes 2097184 | tf_op jit(solution)/shard_map/all_to_all | solution.py:122
  364.8 5.2 %gather_fusion.1 = bf16[256,2048]{1,0:T(8,128)(2,1)} fusion(bf16[512,2048]{1,0:T(8,128)(2,1)} %bitcast.20, s32[1024]{0:T(1024)S(1)} %pad_clamp_fusion), kind=kCustom, calls=%fused_computation.1 | custom fusion | bytes 2098176 | tf_op jit(solution)/shard_map/gather | solution.py:130
  370.0 3.4 reshape.229
  373.4 4.8 %multiply_reduce_fusion = f32[128,2048]{1,0:T(8,128)S(1)} fusion(f32[128,2,2048]{2,1,0:T(2,128)} %reshape.229, f32[128,2]{1,0:T(8,128)S(1)} %copy.19), kind=kLoop, calls=%fused_computation.10 | loop fusion | flops 786432 | bytes 3146752 | tf_op jit(solution)/shard_map/reduce_sum | solution.py:131
  (59 shorter events, 8.2 us)
Async XLA Ops:
  6.5 228.1 %copy-start = (bf16[1,512,2048]{2,1,0:T(8,128)(2,1)S(1)}, bf16[1,512,2048]{2,1,0:T(8,128)(2,1)}, u32[]{:S(2)}) copy-start(bf16[1,512,2048]{2,1,0:T(8,128)(2,1)} %param.23) | copy-start | bytes 6291460
  6.5 49.0 %reduce-scatter.3.cloned.1.call-start = ((), (), s32[]{:S(2)}) async-start(), calls=%async_computation.4 | async-start | bytes 2621440 | tf_op jit(solution)/shard_map/reduce_scatter | solution.py:93
  7.4 11.2 %collective-permute-start = (bf16[2,512]{1,0:T(2,128)(2,1)S(1)}, bf16[2,512]{1,0:T(2,128)(2,1)S(1)}, u32[]{:S(2)}, u32[]{:S(2)}) collective-permute-start(bf16[2,512]{1,0:T(2,128)(2,1)S(1)} %slice.28), channel_id=1, source_target_pairs={{0,4},{4,8},{8,12},{12,16},{16,20},{20,24},{24,28},{1,5},{5,9},{9,... | collective-permute-start | bytes 6152 | tf_op jit(solution)/shard_map/ppermute | solution.py:20
  13.0 5.6 %collective-permute-start.1 = (bf16[2,512]{1,0:T(2,128)(2,1)S(1)}, bf16[2,512]{1,0:T(2,128)(2,1)S(1)}, u32[]{:S(2)}, u32[]{:S(2)}) collective-permute-start(bf16[2,512]{1,0:T(2,128)(2,1)S(1)} %slice.29), channel_id=1, source_target_pairs={{0,4},{4,8},{8,12},{12,16},{16,20},{20,24},{24,28},{1,5},{5,9},{9,... | collective-permute-start | bytes 6152 | tf_op jit(solution)/shard_map/ppermute | solution.py:20
  18.6 37.0 %copy-start.6 = (bf16[128,2048]{1,0:T(8,128)(2,1)S(1)}, bf16[128,2048]{1,0:T(8,128)(2,1)}, u32[]{:S(2)}) copy-start(bf16[128,2048]{1,0:T(8,128)(2,1)} %param.17) | copy-start | bytes 1572868
  18.6 38.3 %copy-start.8 = (f32[2048]{0:T(1024)S(1)}, f32[2048]{0:T(1024)}, u32[]{:S(2)}) copy-start(f32[2048]{0:T(1024)} %param.18) | copy-start | bytes 24580
  23.2 287.8 %reduce-scatter.5.cloned.1.call-start = ((), (), s32[]{:S(2)}) async-start(), calls=%async_computation.5 | async-start | bytes 10485760 | tf_op jit(solution)/shard_map/reduce_scatter | solution.py:114
  115.2 1.3 copy-start.1
  116.5 25.5 %collective-permute-start.2 = (bf16[1,8,64,2048]{3,2,1,0:T(8,128)(2,1)S(1)}, bf16[1,8,64,2048]{3,2,1,0:T(8,128)(2,1)S(1)}, u32[]{:S(2)}, u32[]{:S(2)}) collective-permute-start(bf16[1,8,64,2048]{3,2,1,0:T(8,128)(2,1)S(1)} %bitcast.43), channel_id=1, source_target_pairs={{0,1},{1,2},{2,3},{3,0},{4,5},{5,6},{6,7},{7,4},{8,9},{9,10},{10,1... | collective-permute-start | bytes 6291464 | tf_op jit(solution)/shard_map/ppermute | solution.py:11
  141.9 1.3 copy-start.4
  143.3 25.6 %collective-permute-start.3 = (bf16[1,8,64,2048]{3,2,1,0:T(8,128)(2,1)S(1)}, bf16[1,8,64,2048]{3,2,1,0:T(8,128)(2,1)}, u32[]{:S(2)}, u32[]{:S(2)}) collective-permute-start(bf16[1,8,64,2048]{3,2,1,0:T(8,128)(2,1)S(1)} %collective-permute-done.2), channel_id=1, source_target_pairs={{0,1},{1,2},{2,3},{3,0},{4,5},{5,6},{6,7},{7,4},{8,9},{9,10},{10,1... | collective-permute-start | bytes 6291464 | tf_op jit(solution)/shard_map/ppermute | solution.py:11
  168.8 25.8 %collective-permute-start.4 = (bf16[1,8,64,2048]{3,2,1,0:T(8,128)(2,1)}, bf16[1,8,64,2048]{3,2,1,0:T(8,128)(2,1)}, u32[]{:S(2)}, u32[]{:S(2)}) collective-permute-start(bf16[1,8,64,2048]{3,2,1,0:T(8,128)(2,1)} %collective-permute-done.3), channel_id=1, source_target_pairs={{0,1},{1,2},{2,3},{3,0},{4,5},{5,6},{6,7},{7,4},{8,9},{9,10},{10,1... | collective-permute-start | bytes 6291464 | tf_op jit(solution)/shard_map/ppermute | solution.py:11
  168.8 32.3 %copy-start.5 = (bf16[1,8,64,2048]{3,2,1,0:T(8,128)(2,1)S(1)}, bf16[1,8,64,2048]{3,2,1,0:T(8,128)(2,1)}, u32[]{:S(2)}) copy-start(bf16[1,8,64,2048]{3,2,1,0:T(8,128)(2,1)} %copy-done.4) | copy-start | bytes 6291460
  197.8 4.8 %copy-start.2 = (bf16[1,8,64,2048]{3,2,0,1:T(8,128)(2,1)S(1)}, bf16[1,8,64,2048]{3,2,0,1:T(8,128)(2,1)}, u32[]{:S(2)}) copy-start(bf16[1,8,64,2048]{3,2,0,1:T(8,128)(2,1)} %copy-done.1) | copy-start | bytes 6291460
  213.4 8.4 %copy-start.9 = (bf16[1,2048,512]{2,1,0:T(8,128)(2,1)S(1)}, bf16[1,2048,512]{2,1,0:T(8,128)(2,1)}, u32[]{:S(2)}) copy-start(bf16[1,2048,512]{2,1,0:T(8,128)(2,1)} %param.21) | copy-start | bytes 6291460
  221.8 7.7 %copy-start.3 = (bf16[4,8,64,2048]{3,2,1,0:T(8,128)(2,1)S(1)}, bf16[4,8,64,2048]{3,2,1,0:T(8,128)(2,1)}, u32[]{:S(2)}) copy-start(bf16[4,8,64,2048]{3,2,1,0:T(8,128)(2,1)} %constant_dynamic-slice_fusion) | copy-start | bytes 25165828
  221.8 7.7 %copy-start.10 = (bf16[1,2048,512]{2,1,0:T(8,128)(2,1)S(1)}, bf16[1,2048,512]{2,1,0:T(8,128)(2,1)}, u32[]{:S(2)}) copy-start(bf16[1,2048,512]{2,1,0:T(8,128)(2,1)} %param.22) | copy-start | bytes 6291460
  311.0 53.7 %all-to-all-start.1 = ((bf16[8,64,2048]{2,1,0:T(8,128)(2,1)}), bf16[8,64,2048]{2,1,0:T(8,128)(2,1)}, u32[]{:S(2)}, u32[]{:S(2)}) async-start(bf16[8,64,2048]{2,1,0:T(8,128)(2,1)} %bitcast.47), calls=%async_computation.3 | async-start | bytes 4194304 | tf_op jit(solution)/shard_map/all_to_all | solution.py:122
  370.0 8.3 %copy-start.7 = (bf16[128,2048]{1,0:T(8,128)(2,1)S(1)}, bf16[128,2048]{1,0:T(8,128)(2,1)}, u32[]{:S(2)}) copy-start(bf16[128,2048]{1,0:T(8,128)(2,1)} %reduce-scatter.3.cloned.1.call-done) | copy-start | bytes 1572868
Sparse Core Ops, SparseCore 0:
  23.4 32.1 reduce-scatter.2
  241.5 69.4 reduce-scatter.4
